TPU v7x, 512 devices: a whole 4x4x16 slice. The times are simulated.
512 devices in a mesh: sp: 64 (over z, y), tp: 8 (over x, core).
Axes of the slice: x: 4, y: 4, z: 16, core: 2. Of those that a mesh axis runs over, the one named last changes fastest.
Arguments:
- residual: bfloat16 [8192, 2048], P(('sp', 'tp')), may hold values from -24 to 24
- query_small: bfloat16 [8192, 768], P('sp', 'tp'), may hold values from -64 to 64
- query_large: bfloat16 [8192, 1280], P('sp', 'tp'), may hold values from -64 to 64
- latent: bfloat16 [8192, 256], P('sp'), may hold values from -6 to 6
- rope_key: bfloat16 [8192, 32], P('sp'), may hold values from -48 to 48
- key_up_small: bfloat16 [256, 512], P(None, 'tp'), may hold values from -0.375 to 0.375
- value_up_small: bfloat16 [256, 512], P(None, 'tp'), may hold values from -0.375 to 0.375
- key_up_large: bfloat16 [256, 1024], P(None, 'tp'), may hold values from -0.375 to 0.375
- value_up_large: bfloat16 [256, 1024], P(None, 'tp'), may hold values from -0.375 to 0.375
- out_small: bfloat16 [512, 2048], P('tp'), may hold values from -0.625 to 0.625
- out_large: bfloat16 [1024, 2048], P('tp'), may hold values from -0.625 to 0.625
- norm_gain: bfloat16 [2048], replicated, may hold values from 0.099609375 to 1.8984375
- gate_weight: bfloat16 [2048, 5632], P('sp', 'tp'), may hold values from -0.125 to 0.125
- up_weight: bfloat16 [2048, 5632], P('sp', 'tp'), may hold values from -0.125 to 0.125
- down_weight: bfloat16 [2048, 5632], P('sp', 'tp'), may hold values from -0.21875 to 0.21875
Outputs:
- layer_out: bfloat16 [8192, 2048], P(('sp', 'tp'))
All inputs are finite; a program needn't handle non-finite values.
Results may differ from a plain program's by a relative error of at most 0.017.
Values may be sent and summed in bfloat16 or wider, within the bound.
No kernel may reach another device: no remote copies, remote signals or barrier semaphores. Data moves between devices by JAX's collectives and lax.ppermute only.
A program may use at most 64 MiB of HBM per device.

v0:
```python
import jax
import jax.numpy as jnp
from jax import lax
from jax.sharding import PartitionSpec as P

HEAD_SMALL = 64
HEAD_LARGE = 128
ROPE = 32
big_negative = -1e30
rope_base = 500000.0
norm_eps = 1e-06


def cut_along(shard, dim, count):
    before, after = (shard.shape[:dim], shard.shape[dim + 1 :])
    return jnp.moveaxis(shard.reshape(*before, count, -1, *after), dim, 0)


def sent_and_summed(shard, axis, dim):
    count = lax.axis_size(axis)
    tiles = lax.all_to_all(cut_along(shard, dim, count), axis, 0, 0, tiled=True)
    return jnp.sum(tiles.astype(jnp.float32), axis=0)


def sent_together(arrays, axis, dim, along):
    widths = [a.shape[along] for a in arrays]
    both = jnp.concatenate(arrays, axis=along)
    whole = lax.all_gather(both, axis, axis=dim, tiled=True)
    return tuple(jnp.split(whole, [sum(widths[:k]) for k in range(1, len(widths))], axis=along))


def laid_out(tiles, dim):
    lengths = list(tiles.shape[1:])
    lengths[dim] *= tiles.shape[0]
    return jnp.moveaxis(tiles, 0, dim).reshape(lengths)


def from_everyone(shard, axis):
    copies = jnp.broadcast_to(shard, (lax.axis_size(axis), *shard.shape))
    return lax.all_to_all(copies, axis, split_axis=0, concat_axis=0, tiled=True)


def collect(shard, axis, dim):
    return laid_out(from_everyone(shard, axis), dim)


def rotate(vectors, positions):
    span_width = vectors.shape[-1]
    half_width = span_width // 2
    inverse = 1.0 / rope_base ** (jnp.arange(0, span_width, 2, dtype=jnp.float32) / span_width)
    angles = positions.astype(jnp.float32)[:, None] * inverse[None, :]
    angle_shape = (vectors.shape[0],) + (1,) * (vectors.ndim - 2) + (half_width,)
    cosine = jnp.cos(angles).reshape(angle_shape)
    sine_table = jnp.sin(angles).reshape(angle_shape)
    leading = vectors[..., :half_width].astype(jnp.float32)
    trailing = vectors[..., half_width:].astype(jnp.float32)
    turned = jnp.concatenate(
        [leading * cosine - trailing * sine_table, trailing * cosine + leading * sine_table],
        axis=-1,
    )
    return turned.astype(jnp.bfloat16)


def group_update(
    running, nope_part, turned_query, key_rows, value_rows, turned_key, visible, head_size
):
    maxima, totals, summed = running
    head_count = nope_part.shape[0]
    key_count = key_rows.shape[0]
    key_rows = key_rows.reshape(key_count, head_count, head_size)
    value_rows = value_rows.reshape(key_count, head_count, head_size)
    scores = jnp.einsum("hqe,khe->hqk", nope_part, key_rows, preferred_element_type=jnp.float32)
    scores = scores + jnp.einsum(
        "hqr,kr->hqk", turned_query, turned_key, preferred_element_type=jnp.float32
    )
    scores = scores * (head_size + ROPE) ** (-0.5)
    masked = jnp.where(visible[None, :, :], scores, big_negative)
    new_maxima = jnp.maximum(maxima, jnp.max(masked, axis=2))
    weights = jnp.where(visible[None, :, :], jnp.exp(masked - new_maxima[:, :, None]), 0.0)
    totals = jnp.sum(weights, axis=2)
    summed = jnp.einsum(
        "hqk,khe->hqe", weights.astype(jnp.bfloat16), value_rows, preferred_element_type=jnp.float32
    )
    return (new_maxima, totals, summed)


def finish(running):
    maxima, totals, summed = running
    head_count, row_count, head_size = summed.shape
    result = summed / totals[:, :, None]
    return (
        jnp.transpose(result, (1, 0, 2))
        .reshape(row_count, head_count * head_size)
        .astype(jnp.bfloat16)
    )


def shards(
    residual,
    query_small,
    query_large,
    latent,
    rope_key,
    key_up_small,
    value_up_small,
    key_up_large,
    value_up_large,
    out_small,
    out_large,
    norm_gain,
    gate_weight,
    up_weight,
    down_weight,
):
    row_count = query_small.shape[0]
    first_row = lax.axis_index("sp") * row_count
    query_pos = first_row + jnp.arange(row_count, dtype=jnp.int32)
    heads_small = key_up_small.shape[1] // HEAD_SMALL
    heads_large = key_up_large.shape[1] // HEAD_LARGE

    def split_query(query, head_count, head_size):
        shaped = query.reshape(row_count, head_count, head_size + ROPE)
        nope_part = jnp.transpose(shaped[..., :head_size], (1, 0, 2))
        turned = jnp.transpose(rotate(shaped[..., head_size:], query_pos), (1, 0, 2))
        return (nope_part, turned)

    nope_small, turned_small = split_query(query_small, heads_small, HEAD_SMALL)
    nope_large, turned_large = split_query(query_large, heads_large, HEAD_LARGE)

    def initial(head_count, head_size):
        return (
            jnp.full((head_count, row_count), big_negative, jnp.float32),
            jnp.zeros((head_count, row_count), jnp.float32),
            jnp.zeros((head_count, row_count, head_size), jnp.float32),
        )

    starting = (initial(heads_small, HEAD_SMALL), initial(heads_large, HEAD_LARGE))
    part_latent = lax.all_gather(latent, "sp", axis=0, tiled=True)
    part_rope = lax.all_gather(rope_key, "sp", axis=0, tiled=True)
    key_count = part_latent.shape[0]
    key_pos = jnp.arange(key_count, dtype=jnp.int32)

    def compute(running):
        turned_key = rotate(part_rope, key_pos)
        visible = key_pos[None, :] <= query_pos[:, None]
        key_small = jnp.dot(part_latent, key_up_small, preferred_element_type=jnp.float32).astype(
            jnp.bfloat16
        )
        value_small = jnp.dot(
            part_latent, value_up_small, preferred_element_type=jnp.float32
        ).astype(jnp.bfloat16)
        key_large = jnp.dot(part_latent, key_up_large, preferred_element_type=jnp.float32).astype(
            jnp.bfloat16
        )
        value_large = jnp.dot(
            part_latent, value_up_large, preferred_element_type=jnp.float32
        ).astype(jnp.bfloat16)
        small_state = group_update(
            running[0],
            nope_small,
            turned_small,
            key_small,
            value_small,
            turned_key,
            visible,
            HEAD_SMALL,
        )
        large_state = group_update(
            running[1],
            nope_large,
            turned_large,
            key_large,
            value_large,
            turned_key,
            visible,
            HEAD_LARGE,
        )
        return (small_state, large_state)

    def keep(running):
        return running

    running = lax.cond(jnp.int32(0) <= query_pos[-1], compute, keep, starting)
    attended_small = finish(running[0])
    attended_large = finish(running[1])
    mixed = sent_and_summed(
        (
            jnp.dot(attended_small, out_small, preferred_element_type=jnp.float32)
            + jnp.dot(attended_large, out_large, preferred_element_type=jnp.float32)
        ).astype(jnp.bfloat16),
        "tp",
        0,
    ).astype(jnp.bfloat16)
    stream = (residual.astype(jnp.float32) + mixed.astype(jnp.float32)).astype(jnp.bfloat16)
    as_float = stream.astype(jnp.float32)
    normed = as_float * lax.rsqrt(jnp.mean(as_float * as_float, axis=-1, keepdims=True) + norm_eps)
    normed = (normed * norm_gain.astype(jnp.float32)[None, :]).astype(jnp.bfloat16)
    gate_full, up_full, down_full = sent_together((gate_weight, up_weight, down_weight), "sp", 0, 1)
    piece = collect(normed, "tp", 0)
    gate_part = jnp.dot(piece, gate_full, preferred_element_type=jnp.float32)
    up_part = jnp.dot(piece, up_full, preferred_element_type=jnp.float32)
    hidden = (jax.nn.silu(gate_part) * up_part).astype(jnp.bfloat16)
    channel = sent_and_summed(
        lax.dot_general(
            hidden, down_full, (((1,), (1,)), ((), ())), preferred_element_type=jnp.float32
        ).astype(jnp.bfloat16),
        "tp",
        0,
    ).astype(jnp.bfloat16)
    return (as_float + 0.5 * channel.astype(jnp.float32)).astype(jnp.bfloat16)


def solution(mesh):
    placed = (
        P(("sp", "tp"), None),
        P("sp", "tp"),
        P("sp", "tp"),
        P("sp", None),
        P("sp", None),
        P(None, "tp"),
        P(None, "tp"),
        P(None, "tp"),
        P(None, "tp"),
        P("tp", None),
        P("tp", None),
        P(),
        P("sp", "tp"),
        P("sp", "tp"),
        P("sp", "tp"),
    )
    return jax.shard_map(
        shards, mesh=mesh, in_specs=placed, out_specs=P(("sp", "tp"), None), check_vma=False
    )
```

profile of v0, /device:TPU:1, one launch (start us, length us, event | category | flops | bytes accessed | tf_op | source)
XLA Modules:
  0.0 348.7 jit_solution(13543055869742643674)
XLA Ops:
  6.5 0.0 copy-start
  6.5 0.0 all-gather.3.cloned.1.call-start
  6.5 0.7 all-gather.3.cloned.1.call-update
  7.3 0.0 all-gather.5.cloned.1.call-start
  7.3 1.6 concatenate.47
  8.9 0.0 all-gather.5.cloned.1.call-update
  8.9 0.6 slice.35
  10.2 0.9 fusion.87
  11.1 86.3 %all_gather.10 = bf16[8192,32]{0,1:T(8,128)(2,1)S(1)} all-gather(bf16[128,32]{0,1:T(8,128)(2,1)} %param.21), channel_id=1, replica_groups=mesh['sp'=64,'tp'=8] {'sp'}, dimensions={0}, use_global_device_ids=true | all-gather | bytes 532480 | tf_op jit(solution)/shard_map/all_gather | solution.py:139
  97.3 54.7 %all-gather.3.cloned.1.call-done = bf16[8192,256]{1,0:T(8,128)(2,1)} async-done(((bf16[128,256]{1,0:T(8,128)(2,1)}), bf16[8192,256]{1,0:T(8,128)(2,1)}) %all-gather.3.cloned.1.call-update) | async-done | bytes 4194320 | tf_op jit(solution)/shard_map/all_gather | solution.py:138
  152.0 0.0 copy-start.2
  152.0 49.8 %conditional.1 = (f32[1,128]{1,0:T(1,128)S(1)}, f32[1,128,64]{1,2,0:T(8,128)S(1)}, f32[1,128]{1,0:T(1,128)S(1)}, f32[1,128,128]{2,1,0:T(8,128)S(1)}) conditional(s32[]{:T(128)} %bitcast.10, () %tuple.13, (s32[8192]{0:T(1024)S(1)}, s32[128]{0:T(128)S(1)}, bf16[8192,256]{1,0:T(8,128)(2,1)}, bf16[256,64]{0,1:T(8,128)(2,1)}, ...), branch_computations={%region_0.0_spmd, %region_1.6_spmd} | conditional | flops 2583461632 | bytes 62645008 | solution.py:183
  152.0 6.2 %fusion.20 = f32[8192,128]{1,0:T(8,128)} fusion(bf16[8192,256]{1,0:T(8,128)(2,1)} %get-tuple-element.39, bf16[256,64]{0,1:T(8,128)(2,1)} %get-tuple-element.104, bf16[128,1,96]{0,2,1:T(8,128)(2,1)} %get-tuple-element.41), kind=kOutput, calls=%fused_computation.26 | convolution fusion | flops 403177472 | bytes 8437760 | tf_op jit(solution)/shard_map/cond/branch_1_fun/hqe,khe->hqk/dot_general | solution.py:72
  158.3 7.2 %fusion.28 = (bf16[8192,16]{0,1:T(8,128)(2,1)S(1)}, bf16[8192,16]{0,1:T(8,128)(2,1)S(1)}) fusion(f32[8192]{0:T(1024)S(1)} %convert_element_type.101, f32[16]{0:T(128)S(1)} %negate_power_fusion, f32[8192]{0:T(1024)S(1)} %convert_element_type.99, bf16[8192,32]{0,1:T(8,128)(2,1)S(1)} %get-tuple-element.42, f32[8192]{0:T(1024)S(1)} %convert_element_type.103, ...), kind=kLoop, calls=%fused_computation.34 | loop fusion | flops 1835008 | bytes 1179712 | tf_op jit(solution)/shard_map/convert.2
  165.4 0.0 copy-start.4
  165.5 0.0 copy-start.3
  165.5 5.8 %fusion.93 = (f32[128]{0:T(128)S(1)}, f32[128,8192]{0,1:T(8,128)}) fusion(f32[8192,128]{1,0:T(8,128)} %fusion.20, bf16[1,128,32]{1,2,0:T(8,128)(2,1)S(1)} %get-tuple-element.111, bf16[8192,16]{0,1:T(8,128)(2,1)S(1)} %get-tuple-element.120, bf16[8192,16]{0,1:T(8,128)(2,1)S(1)} %get-tuple-element.119, s32[128]{0:T(128)S(1)} %get-tuple-element.38, ...), kind=kOutput, calls=%fused_computation.110 | convolution fusion | flops 73400192 | bytes 8954880 | tf_op jit(solution)/shard_map/cond/branch_1_fun/hqr,kr->hqk/dot_general | solution.py:73
  171.2 0.0 copy-done.4
  171.2 0.1 copy.38
  171.4 0.0 copy-done.3
  171.4 6.3 %fusion.19 = f32[8192,128]{1,0:T(8,128)} fusion(bf16[8192,256]{1,0:T(8,128)(2,1)} %get-tuple-element.39, bf16[256,128]{1,0:T(8,128)(2,1)S(1)} %copy-done.3, bf16[128,1,160]{2,0,1:T(8,128)(2,1)S(1)} %copy.38), kind=kOutput, calls=%fused_computation.25 | convolution fusion | flops 806354944 | bytes 8486912 | tf_op jit(solution)/shard_map/cond/branch_1_fun/hqe,khe->hqk/dot_general | solution.py:72
  177.7 5.8 %fusion.92 = (f32[128]{0:T(128)S(1)}, f32[128,8192]{0,1:T(8,128)}) fusion(f32[8192,128]{1,0:T(8,128)} %fusion.19, bf16[1,128,32]{1,2,0:T(8,128)(2,1)S(1)} %get-tuple-element.115, bf16[8192,16]{0,1:T(8,128)(2,1)S(1)} %get-tuple-element.120, bf16[8192,16]{0,1:T(8,128)(2,1)S(1)} %get-tuple-element.119, s32[128]{0:T(128)S(1)} %get-tuple-element.38, ...), kind=kOutput, calls=%fused_computation.109 | convolution fusion | flops 73400192 | bytes 8954880 | tf_op jit(solution)/shard_map/cond/branch_1_fun/hqr,kr->hqk/dot_general | solution.py:73
  183.5 0.0 copy-done.6
  183.5 0.0 copy-start.7
  183.5 6.0 %fusion.21 = f32[1,128,128]{2,1,0:T(8,128)S(1)} fusion(bf16[8192,256]{1,0:T(8,128)(2,1)} %get-tuple-element.39, bf16[256,128]{1,0:T(8,128)(2,1)S(1)} %copy-done.6, f32[128,8192]{0,1:T(8,128)} %get-tuple-element.122, f32[128]{0:T(128)S(1)} %get-tuple-element.125, s32[128]{0:T(128)S(1)} %get-tuple-element.38, s32[8192]{0:T(1024)S(1)} %get-tuple-element.46), kind=kOutput, calls=%fused_computation.27 | convolution fusion | flops 810549248 | bytes 8553472 | tf_op jit(solution)/shard_map/cond/branch_1_fun/hqk,khe->hqe/dot_general | solution.py:81
  189.5 0.0 copy-done.7
  189.5 5.7 %fusion.24 = f32[1,128,64]{1,2,0:T(8,128)S(1)} fusion(f32[128,8192]{0,1:T(8,128)} %get-tuple-element.124, f32[128]{0:T(128)S(1)} %get-tuple-element.126, s32[128]{0:T(128)S(1)} %get-tuple-element.38, s32[8192]{0:T(1024)S(1)} %get-tuple-element.46, bf16[8192,256]{1,0:T(8,128)(2,1)} %get-tuple-element.39, bf16[256,64]{0,1:T(8,128)(2,1)S(1)} %copy-done.7), kind=kOutput, calls=%fused_computation.28 | convolution fusion | flops 407371776 | bytes 8487936 | tf_op jit(solution)/shard_map/cond/branch_1_fun/hqk,khe->hqe/dot_general | solution.py:81
  195.2 6.6 %fusion.9 = (f32[128]{0:T(128)S(1)}, f32[128]{0:T(128)S(1)}) fusion(f32[128,8192]{0,1:T(8,128)} %get-tuple-element.122, f32[128]{0:T(128)S(1)} %get-tuple-element.125, s32[128]{0:T(128)S(1)} %get-tuple-element.38, s32[8192]{0:T(1024)S(1)} %get-tuple-element.46, f32[128,8192]{0,1:T(8,128)} %get-tuple-element.124, f32[128]{0:T(128)S(1)} %get-tuple-element.126), kind=kLoop, calls=%fused_computation.17 | loop fusion | flops 7339776 | bytes 8423936 | tf_op jit(solution)/shard_map/cond/branch_1_fun/reduce_sum | solution.py:80
  201.8 0.0 copy-start.5
  201.8 0.0 copy-start.1
  201.8 0.0 copy-done.2
  201.8 0.3 fusion.68
  202.2 0.0 copy-done
  202.2 1.2 fusion.45
  203.3 14.8 %all-to-all-start = ((bf16[8,16,2048]{2,1,0:T(8,128)(2,1)}), bf16[8,16,2048]{2,1,0:T(8,128)(2,1)S(1)}, u32[]{:S(2)}, u32[]{:S(2)}) async-start(bf16[8,16,2048]{2,1,0:T(8,128)(2,1)} %bitcast.21), calls=%async_computation | async-start | bytes 1048576 | tf_op jit(solution)/shard_map/all_to_all | solution.py:21
  218.1 0.0 copy-done.5
  218.1 9.3 %all-to-all-done = bf16[8,16,2048]{2,1,0:T(8,128)(2,1)S(1)} async-done(((bf16[8,16,2048]{2,1,0:T(8,128)(2,1)}), bf16[8,16,2048]{2,1,0:T(8,128)(2,1)S(1)}, u32[]{:S(2)}, u32[]{:S(2)}) %all-to-all-start) | async-done | bytes 524320 | tf_op jit(solution)/shard_map/all_to_all | solution.py:21
  227.5 0.1 reduce_sum.55
  227.5 0.0 copy-done.1
  227.5 0.1 fusion.63
  227.7 0.1 fusion.65
  227.8 12.9 %all_to_all.15 = bf16[8,16,2048]{2,1,0:T(8,128)(2,1)S(1)} all-to-all(bf16[8,16,2048]{2,1,0:T(8,128)(2,1)S(1)} %broadcast_in_dim.17), channel_id=1, replica_groups=mesh['sp'=64,'tp'=8] {'tp'}, dimensions={0} | all-to-all | bytes 1048576 | tf_op jit(solution)/shard_map/all_to_all | solution.py:40
  240.7 68.3 %all-gather.5.cloned.1.call-done = bf16[2048,2112]{1,0:T(8,128)(2,1)} async-done(((bf16[32,2112]{1,0:T(8,128)(2,1)}), bf16[2048,2112]{1,0:T(8,128)(2,1)}) %all-gather.5.cloned.1.call-update) | async-done | bytes 8650768 | tf_op jit(solution)/shard_map/all_gather | solution.py:28
  309.0 3.2 fusion.43
  312.2 7.2 %fusion.46 = bf16[128,2048]{1,0:T(8,128)(2,1)S(1)} fusion(bf16[2048,2112]{1,0:T(8,128)(2,1)} %all-gather.5.cloned.1.call-done, bf16[128,2048]{1,0:T(8,128)(2,1)S(1)} %bitcast.67, f32[128,704]{0,1:T(8,128)S(1)} %fusion.43), kind=kOutput, calls=%fused_computation.58 | convolution fusion | flops 739000320 | bytes 7700480 | tf_op jit(solution)/shard_map/dot_general | solution.py:204
  319.5 21.6 %all_to_all.16 = bf16[8,16,2048]{2,1,0:T(8,128)(2,1)S(1)} all-to-all(bf16[8,16,2048]{2,1,0:T(8,128)(2,1)S(1)} %bitcast.68), channel_id=1, replica_groups=mesh['sp'=64,'tp'=8] {'tp'}, dimensions={0} | all-to-all | bytes 1048576 | tf_op jit(solution)/shard_map/all_to_all | solution.py:21
  341.1 0.1 reduce_sum.57
  341.2 0.7 fusion.66
  (15 shorter events, 0.1 us)
Async XLA Ops:
  6.5 195.6 %copy-start = (bf16[128,2048]{1,0:T(8,128)(2,1)S(1)}, bf16[128,2048]{1,0:T(8,128)(2,1)}, u32[]{:S(2)}) copy-start(bf16[128,2048]{1,0:T(8,128)(2,1)} %param.27) | copy-start | bytes 1572868
  6.5 145.5 %all-gather.3.cloned.1.call-start = ((), (), s32[]{:S(2)}) async-start(), calls=%async_computation.3 | async-start | bytes 4259840 | tf_op jit(solution)/shard_map/all_gather | solution.py:138
  7.3 301.8 %all-gather.5.cloned.1.call-start = ((), (), s32[]{:S(2)}) async-start(), calls=%async_computation.4 | async-start | bytes 9052160 | tf_op jit(solution)/shard_map/all_gather | solution.py:28
  152.0 49.8 %copy-start.2 = (bf16[64,2048]{1,0:T(8,128)(2,1)S(1)}, bf16[64,2048]{1,0:T(8,128)(2,1)}, u32[]{:S(2)}) copy-start(bf16[64,2048]{1,0:T(8,128)(2,1)} %param.26) | copy-start | bytes 786436
  165.4 5.8 %copy-start.4 = (bf16[128,1,160]{0,2,1:T(8,128)(2,1)S(1)}, bf16[128,1,160]{0,2,1:T(8,128)(2,1)}, u32[]{:S(2)}) copy-start(bf16[128,1,160]{0,2,1:T(8,128)(2,1)} %get-tuple-element.114) | copy-start | bytes 122884 | tf_op jit(solution)/shard_map/cond
  165.5 5.9 %copy-start.3 = (bf16[256,128]{1,0:T(8,128)(2,1)S(1)}, bf16[256,128]{1,0:T(8,128)(2,1)}, u32[]{:S(2)}) copy-start(bf16[256,128]{1,0:T(8,128)(2,1)} %get-tuple-element.67) | copy-start | bytes 196612 | tf_op jit(solution)/shard_map/cond
  177.7 5.8 %copy-start.6 = (bf16[256,128]{1,0:T(8,128)(2,1)S(1)}, bf16[256,128]{1,0:T(8,128)(2,1)}, u32[]{:S(2)}) copy-start(bf16[256,128]{1,0:T(8,128)(2,1)} %get-tuple-element.68) | copy-start | bytes 196612 | tf_op jit(solution)/shard_map/cond
  183.5 6.0 %copy-start.7 = (bf16[256,64]{0,1:T(8,128)(2,1)S(1)}, bf16[256,64]{0,1:T(8,128)(2,1)}, u32[]{:S(2)}) copy-start(bf16[256,64]{0,1:T(8,128)(2,1)} %get-tuple-element.112) | copy-start | bytes 98308 | tf_op jit(solution)/shard_map/cond
  201.8 16.3 %copy-start.5 = (bf16[2048]{0:T(1024)(128)(2,1)S(1)}, bf16[2048]{0:T(1024)(128)(2,1)}, u32[]{:S(2)}) copy-start(bf16[2048]{0:T(1024)(128)(2,1)} %param.28) | copy-start | bytes 12292
  201.8 25.7 %copy-start.1 = (bf16[16,2048]{1,0:T(8,128)(2,1)S(1)}, bf16[16,2048]{1,0:T(8,128)(2,1)}, u32[]{:S(2)}) copy-start(bf16[16,2048]{1,0:T(8,128)(2,1)} %param.17) | copy-start | bytes 196612
  203.3 24.1 %all-to-all-start = ((bf16[8,16,2048]{2,1,0:T(8,128)(2,1)}), bf16[8,16,2048]{2,1,0:T(8,128)(2,1)S(1)}, u32[]{:S(2)}, u32[]{:S(2)}) async-start(bf16[8,16,2048]{2,1,0:T(8,128)(2,1)} %bitcast.21), calls=%async_computation | async-start | bytes 1048576 | tf_op jit(solution)/shard_map/all_to_all | solution.py:21
Sparse Core Ops, SparseCore 0:
  10.3 141.7 all-gather.2
  155.0 154.0 all-gather.4
where the time goes:
time: 349 us
  waiting for transfers between devices  133 us (38%)
  blocking collectives  121 us (35%)
  matrix products  47.6 us (14%)
  other arithmetic  15.8 us (5%)
  starting transfers between devices  14.8 us (4%)
  between operations  14.2 us (4%)
    all_gather x1, blocking collectives, shards(): part_rope = lax.all_gather(rope_key, 'sp', axis=0, tiled=True)  86.3 us
    all_gather x1, waiting for transfers between devices, sent_together(): whole = lax.all_gather(both, axis, axis=dim, tiled=True)  68.3 us
    all_gather x1, waiting for transfers between devices, shards(): part_latent = lax.all_gather(latent, 'sp', axis=0, tiled=True)  54.7 us
    all_to_all x1, blocking collectives, sent_and_summed(): tiles = lax.all_to_all(cut_along(shard, dim, count), axis, 0, 0, tiled=True)  21.6 us
    all_to_all x1, starting transfers between devices, sent_and_summed(): tiles = lax.all_to_all(cut_along(shard, dim, count), axis, 0, 0, tiled=True)  14.8 us
    all_to_all x1, blocking collectives, from_everyone(): return lax.all_to_all(copies, axis, split_axis=0, concat_axis=0, tiled=True)  12.9 us
    dot_general x2, matrix products, group_update(): jnp.einsum('hqe,khe->hqk', nope_part, key_rows, preferred_element_type=jn...  12.5 us
    dot_general x2, matrix products, group_update(): jnp.einsum('hqk,khe->hqe', weights.astype(jnp.bfloat16), value_rows, pref...  11.7 us
  transfers between devices with their start and end apart: 3, of which 3 were waited for; matrix products, arithmetic and copies ran while one was open for 16% of the time, Pallas kernels for 0%

commit v1 on v0

--- a/solution.py
+++ b/solution.py
@@ -2,6 +2,7 @@
 import jax.numpy as jnp
 from jax import lax
 from jax.sharding import PartitionSpec as P
+from jax.lax import all_to_all, psum
 
 HEAD_SMALL = 64
 HEAD_LARGE = 128
@@ -9,6 +10,12 @@
 big_negative = -1e30
 rope_base = 500000.0
 norm_eps = 1e-06
+
+
+def unit_deliver(row_data, shard_axis):
+    return jnp.concatenate(
+        all_to_all(jnp.stack([row_data] * psum(1, shard_axis), axis=0), shard_axis, 0, 0), 0
+    )
 
 
 def cut_along(shard, dim, count):
@@ -135,7 +142,7 @@
         )
 
     starting = (initial(heads_small, HEAD_SMALL), initial(heads_large, HEAD_LARGE))
-    part_latent = lax.all_gather(latent, "sp", axis=0, tiled=True)
+    part_latent = unit_deliver(latent, "sp")
     part_rope = lax.all_gather(rope_key, "sp", axis=0, tiled=True)
     key_count = part_latent.shape[0]
     key_pos = jnp.arange(key_count, dtype=jnp.int32)

time: 349 us -> 448 us (1.28)
  blocking collectives: 121 us -> 295 us
  waiting for transfers between devices: 133 us -> 18.7 us
  starting transfers between devices: 14.8 us -> 50.6 us
    all_gather x1, blocking collectives: 86.3 us -> 282 us  [shards(): part_rope = lax.all_gather(rope_key, 'sp', axis=0, tiled=True)]
    all_gather x1, waiting for transfers between devices: 68.3 us -> 0.01 us  [sent_together(): whole = lax.all_gather(both, axis, axis=dim, tiled=True)]
    all_gather x1 -> x0, waiting for transfers between devices: 54.7 us -> none  [shards(): part_latent = lax.all_gather(latent, 'sp', axis=0, tiled=True)]
    all_to_all x0 -> x2, starting transfers between devices: none -> 24 us  [the longest x1 19.7 us: unit_deliver(): all_to_all(jnp.stack([row_data] * psum(1, shard_axis), axis=0), shard_axi...]
    all_to_all x1 -> x0, blocking collectives: 12.9 us -> none  [from_everyone(): return lax.all_to_all(copies, axis, split_axis=0, concat_axis=0, tiled=True)]
    all_to_all x1, starting transfers between devices: 14.8 us -> 26.6 us  [sent_and_summed(): tiles = lax.all_to_all(cut_along(shard, dim, count), axis, 0, 0, tiled=True)]
    all_to_all x0 -> x2, waiting for transfers between devices: none -> 9.38 us  [the longest x1 9.38 us: from_everyone(): return lax.all_to_all(copies, axis, split_axis=0, concat_axis=0, tiled=True)]
    all_to_all x1, blocking collectives: 21.6 us -> 12.7 us  [sent_and_summed(): tiles = lax.all_to_all(cut_along(shard, dim, count), axis, 0, 0, tiled=True)]
  transfers between devices with their start and end apart: 3 -> 4, of which waited for: 3 -> 2; matrix products, arithmetic and copies ran while one was open for 16% -> 12% of each run, Pallas kernels for 0% -> 0%
where the time goes in v1:
time: 448 us; the launch traced here: 447 us
  blocking collectives  295 us (66%)
  starting transfers between devices  50.6 us (11%)
  matrix products  47.5 us (11%)
  waiting for transfers between devices  18.7 us (4%)
  other arithmetic  15 us (3%)
  between operations  14.3 us (3%)
  local copies, waits for them, and re-layouts  5.73 us (1%)
    all_gather x1, blocking collectives, shards(): part_rope = lax.all_gather(rope_key, 'sp', axis=0, tiled=True)  282 us
    all_to_all x1, starting transfers between devices, sent_and_summed(): tiles = lax.all_to_all(cut_along(shard, dim, count), axis, 0, 0, tiled=True)  26.6 us
    all_to_all x1, starting transfers between devices, unit_deliver(): all_to_all(jnp.stack([row_data] * psum(1, shard_axis), axis=0), shard_axi...  19.7 us
    all_to_all x1, blocking collectives, sent_and_summed(): tiles = lax.all_to_all(cut_along(shard, dim, count), axis, 0, 0, tiled=True)  12.7 us
    dot_general x2, matrix products, group_update(): jnp.einsum('hqe,khe->hqk', nope_part, key_rows, preferred_element_type=jn...  12.5 us
    dot_general x2, matrix products, group_update(): jnp.einsum('hqk,khe->hqe', weights.astype(jnp.bfloat16), value_rows, pref...  11.6 us
    dot_general x2, matrix products, group_update(): jnp.einsum('hqr,kr->hqk', turned_query, turned_key, preferred_element_typ...  11.5 us
    all_to_all x1, waiting for transfers between devices, from_everyone(): return lax.all_to_all(copies, axis, split_axis=0, concat_axis=0, tiled=True)  9.38 us
  transfers between devices with their start and end apart: 4, of which 2 were waited for; matrix products, arithmetic and copies ran while one was open for 12% of the time, Pallas kernels for 0%

profile of v1, /device:TPU:1, one launch (start us, length us, event | category | flops | bytes accessed | tf_op | source)
XLA Modules:
  0.0 446.9 jit_solution(10610583475535515243)
XLA Ops:
  6.5 0.0 copy-start
  6.5 3.3 stack.2
  9.9 0.0 copy-start.9
  9.9 0.0 copy-start.10
  9.9 0.0 copy-start.3
  9.9 0.0 copy-start.8
  9.9 0.0 copy-start.12
  9.9 0.0 copy-start.13
  9.9 19.7 %all-to-all-start = ((bf16[64,128,256]{2,1,0:T(8,128)(2,1)}), bf16[64,128,256]{2,1,0:T(8,128)(2,1)}, u32[]{:S(2)}, u32[]{:S(2)}) async-start(bf16[64,128,256]{2,1,0:T(8,128)(2,1)} %stack.2), calls=%async_computation | async-start | bytes 8388608 | tf_op jit(solution)/shard_map/all_to_all | solution.py:17
  29.6 0.0 all-gather.2.cloned.1.call-start
  29.7 0.0 copy-done.5
  29.7 0.0 copy-done.6
  29.7 0.0 copy-done.7
  29.7 0.8 concatenate.47
  30.5 0.0 all-gather.2.cloned.1.call-update
  30.5 0.6 slice.35
  31.8 0.1 fusion.87
  31.9 0.0 copy-done.10
  31.9 282.0 %all_gather.6 = bf16[8192,32]{0,1:T(8,128)(2,1)S(1)} all-gather(bf16[128,32]{0,1:T(8,128)(2,1)S(1)} %copy-done.10), channel_id=1, replica_groups=mesh['sp'=64,'tp'=8] {'sp'}, dimensions={0}, use_global_device_ids=true | all-gather | bytes 532480 | tf_op jit(solution)/shard_map/all_gather | solution.py:146
  314.0 0.0 all-to-all-done
  314.0 0.0 copy-start.2
  314.0 49.8 %conditional.1 = (f32[1,128]{1,0:T(1,128)S(1)}, f32[1,128,64]{1,2,0:T(8,128)S(1)}, f32[1,128]{1,0:T(1,128)S(1)}, f32[1,128,128]{2,1,0:T(8,128)S(1)}) conditional(s32[]{:T(128)} %bitcast.11, () %tuple.13, (s32[8192]{0:T(1024)S(1)}, s32[128]{0:T(128)S(1)}, bf16[64,128,256]{2,1,0:T(8,128)(2,1)}, bf16[256,64]{0,1:T(8,128)(2,1)S(1)}, ...), branch_computations={%region_0.0_spmd, %region_1.6_spmd} | conditional | flops 2583461632 | bytes 61825696 | solution.py:190
  314.2 6.2 %fusion.20 = f32[8192,128]{1,0:T(8,128)} fusion(bf16[8192,256]{1,0:T(8,128)(2,1)} %bitcast, bf16[256,64]{0,1:T(8,128)(2,1)S(1)} %get-tuple-element.105, bf16[128,1,96]{0,2,1:T(8,128)(2,1)S(1)} %get-tuple-element.42), kind=kOutput, calls=%fused_computation.26 | convolution fusion | flops 403177472 | bytes 8437760 | tf_op jit(solution)/shard_map/cond/branch_1_fun/hqe,khe->hqk/dot_general | solution.py:79
  320.5 7.2 %fusion.28 = (bf16[8192,16]{0,1:T(8,128)(2,1)S(1)}, bf16[8192,16]{0,1:T(8,128)(2,1)S(1)}) fusion(f32[8192]{0:T(1024)S(1)} %convert_element_type.101, f32[16]{0:T(128)S(1)} %negate_power_fusion, f32[8192]{0:T(1024)S(1)} %convert_element_type.99, bf16[8192,32]{0,1:T(8,128)(2,1)S(1)} %get-tuple-element.43, f32[8192]{0:T(1024)S(1)} %convert_element_type.103, ...), kind=kLoop, calls=%fused_computation.34 | loop fusion | flops 1835008 | bytes 1179712 | tf_op jit(solution)/shard_map/convert.2
  327.6 5.8 %fusion.93 = (f32[128]{0:T(128)S(1)}, f32[128,8192]{0,1:T(8,128)}) fusion(f32[8192,128]{1,0:T(8,128)} %fusion.20, bf16[1,128,32]{1,2,0:T(8,128)(2,1)S(1)} %get-tuple-element.112, bf16[8192,16]{0,1:T(8,128)(2,1)S(1)} %get-tuple-element.121, bf16[8192,16]{0,1:T(8,128)(2,1)S(1)} %get-tuple-element.120, s32[128]{0:T(128)S(1)} %get-tuple-element.39, ...), kind=kOutput, calls=%fused_computation.110 | convolution fusion | flops 73400192 | bytes 8954880 | tf_op jit(solution)/shard_map/cond/branch_1_fun/hqr,kr->hqk/dot_general | solution.py:80
  333.4 0.1 copy.38
  333.5 6.3 %fusion.19 = f32[8192,128]{1,0:T(8,128)} fusion(bf16[8192,256]{1,0:T(8,128)(2,1)} %bitcast, bf16[256,128]{1,0:T(8,128)(2,1)S(1)} %get-tuple-element.68, bf16[128,1,160]{2,0,1:T(8,128)(2,1)S(1)} %copy.38), kind=kOutput, calls=%fused_computation.25 | convolution fusion | flops 806354944 | bytes 8486912 | tf_op jit(solution)/shard_map/cond/branch_1_fun/hqe,khe->hqk/dot_general | solution.py:79
  339.8 5.8 %fusion.92 = (f32[128]{0:T(128)S(1)}, f32[128,8192]{0,1:T(8,128)}) fusion(f32[8192,128]{1,0:T(8,128)} %fusion.19, bf16[1,128,32]{1,2,0:T(8,128)(2,1)S(1)} %get-tuple-element.116, bf16[8192,16]{0,1:T(8,128)(2,1)S(1)} %get-tuple-element.121, bf16[8192,16]{0,1:T(8,128)(2,1)S(1)} %get-tuple-element.120, s32[128]{0:T(128)S(1)} %get-tuple-element.39, ...), kind=kOutput, calls=%fused_computation.109 | convolution fusion | flops 73400192 | bytes 8954880 | tf_op jit(solution)/shard_map/cond/branch_1_fun/hqr,kr->hqk/dot_general | solution.py:80
  345.6 6.0 %fusion.21 = f32[1,128,128]{2,1,0:T(8,128)S(1)} fusion(bf16[8192,256]{1,0:T(8,128)(2,1)} %bitcast, bf16[256,128]{1,0:T(8,128)(2,1)S(1)} %get-tuple-element.69, f32[128,8192]{0,1:T(8,128)} %get-tuple-element.123, f32[128]{0:T(128)S(1)} %get-tuple-element.126, s32[128]{0:T(128)S(1)} %get-tuple-element.39, s32[8192]{0:T(1024)S(1)} %get-tuple-element.47), kind=kOutput, calls=%fused_computation.27 | convolution fusion | flops 810549248 | bytes 8553472 | tf_op jit(solution)/shard_map/cond/branch_1_fun/hqk,khe->hqe/dot_general | solution.py:88
  351.5 5.6 %fusion.24 = f32[1,128,64]{1,2,0:T(8,128)S(1)} fusion(f32[128,8192]{0,1:T(8,128)} %get-tuple-element.125, f32[128]{0:T(128)S(1)} %get-tuple-element.127, s32[128]{0:T(128)S(1)} %get-tuple-element.39, s32[8192]{0:T(1024)S(1)} %get-tuple-element.47, bf16[8192,256]{1,0:T(8,128)(2,1)} %bitcast, bf16[256,64]{0,1:T(8,128)(2,1)S(1)} %get-tuple-element.113), kind=kOutput, calls=%fused_computation.28 | convolution fusion | flops 407371776 | bytes 8487936 | tf_op jit(solution)/shard_map/cond/branch_1_fun/hqk,khe->hqe/dot_general | solution.py:88
  357.2 6.6 %fusion.9 = (f32[128]{0:T(128)S(1)}, f32[128]{0:T(128)S(1)}) fusion(f32[128,8192]{0,1:T(8,128)} %get-tuple-element.123, f32[128]{0:T(128)S(1)} %get-tuple-element.126, s32[128]{0:T(128)S(1)} %get-tuple-element.39, s32[8192]{0:T(1024)S(1)} %get-tuple-element.47, f32[128,8192]{0,1:T(8,128)} %get-tuple-element.125, f32[128]{0:T(128)S(1)} %get-tuple-element.127), kind=kLoop, calls=%fused_computation.17 | loop fusion | flops 7339776 | bytes 8423936 | tf_op jit(solution)/shard_map/cond/branch_1_fun/reduce_sum | solution.py:87
  363.8 0.0 copy-start.11
  363.8 0.0 copy-start.1
  363.8 0.3 fusion.68
  364.2 1.2 fusion.45
  365.4 26.6 %all-to-all-start.1 = ((bf16[8,16,2048]{2,1,0:T(8,128)(2,1)}), bf16[8,16,2048]{2,1,0:T(8,128)(2,1)S(1)}, u32[]{:S(2)}, u32[]{:S(2)}) async-start(bf16[8,16,2048]{2,1,0:T(8,128)(2,1)} %bitcast.22), calls=%async_computation.1 | async-start | bytes 1048576 | tf_op jit(solution)/shard_map/all_to_all | solution.py:28
  391.9 9.3 %all-to-all-done.1 = bf16[8,16,2048]{2,1,0:T(8,128)(2,1)S(1)} async-done(((bf16[8,16,2048]{2,1,0:T(8,128)(2,1)}), bf16[8,16,2048]{2,1,0:T(8,128)(2,1)S(1)}, u32[]{:S(2)}, u32[]{:S(2)}) %all-to-all-start.1) | async-done | bytes 524320 | tf_op jit(solution)/shard_map/all_to_all | solution.py:28
  401.3 0.1 reduce_sum.55
  401.3 0.1 fusion.63
  401.5 0.1 fusion.65
  401.6 0.9 broadcast_in_dim.17
  402.5 4.4 all-to-all-start.2
  406.8 9.4 %all-to-all-done.2 = bf16[8,16,2048]{2,1,0:T(8,128)(2,1)S(1)} async-done(((bf16[8,16,2048]{2,1,0:T(8,128)(2,1)}), bf16[8,16,2048]{2,1,0:T(8,128)(2,1)S(1)}, u32[]{:S(2)}, u32[]{:S(2)}) %all-to-all-start.2) | async-done | bytes 524320 | tf_op jit(solution)/shard_map/all_to_all | solution.py:47
  416.2 3.2 fusion.43
  419.4 7.2 %fusion.46 = bf16[128,2048]{1,0:T(8,128)(2,1)S(1)} fusion(bf16[2048,2112]{1,0:T(8,128)(2,1)} %all-gather.2.cloned.1.call-done, bf16[128,2048]{1,0:T(8,128)(2,1)S(1)} %bitcast.68, f32[128,704]{0,1:T(8,128)S(1)} %fusion.43), kind=kOutput, calls=%fused_computation.58 | convolution fusion | flops 739000320 | bytes 7700480 | tf_op jit(solution)/shard_map/dot_general | solution.py:211
  426.7 12.7 %all_to_all.20 = bf16[8,16,2048]{2,1,0:T(8,128)(2,1)S(1)} all-to-all(bf16[8,16,2048]{2,1,0:T(8,128)(2,1)S(1)} %bitcast.69), channel_id=1, replica_groups=mesh['sp'=64,'tp'=8] {'tp'}, dimensions={0} | all-to-all | bytes 1048576 | tf_op jit(solution)/shard_map/all_to_all | solution.py:28
  439.4 0.1 reduce_sum.57
  439.4 0.7 fusion.66
  (28 shorter events, 0.1 us)
Async XLA Ops:
  6.5 357.6 %copy-start = (bf16[128,2048]{1,0:T(8,128)(2,1)S(1)}, bf16[128,2048]{1,0:T(8,128)(2,1)}, u32[]{:S(2)}) copy-start(bf16[128,2048]{1,0:T(8,128)(2,1)} %param.27) | copy-start | bytes 1572868
  9.9 19.8 %copy-start.5 = (bf16[32,704]{1,0:T(8,128)(2,1)S(1)}, bf16[32,704]{1,0:T(8,128)(2,1)}, u32[]{:S(2)}) copy-start(bf16[32,704]{1,0:T(8,128)(2,1)} %param.29) | copy-start | bytes 135172
  9.9 19.8 %copy-start.6 = (bf16[32,704]{1,0:T(8,128)(2,1)S(1)}, bf16[32,704]{1,0:T(8,128)(2,1)}, u32[]{:S(2)}) copy-start(bf16[32,704]{1,0:T(8,128)(2,1)} %param.30) | copy-start | bytes 135172
  9.9 19.8 %copy-start.7 = (bf16[32,704]{1,0:T(8,128)(2,1)S(1)}, bf16[32,704]{1,0:T(8,128)(2,1)}, u32[]{:S(2)}) copy-start(bf16[32,704]{1,0:T(8,128)(2,1)} %param.31) | copy-start | bytes 135172
  9.9 21.9 %copy-start.4 = (bf16[128,160]{0,1:T(8,128)(2,1)S(1)}, bf16[128,160]{0,1:T(8,128)(2,1)}, u32[]{:S(2)}) copy-start(bf16[128,160]{0,1:T(8,128)(2,1)} %param.19) | copy-start | bytes 122884
  9.9 21.9 %copy-start.9 = (bf16[128,96]{0,1:T(8,128)(2,1)S(1)}, bf16[128,96]{0,1:T(8,128)(2,1)}, u32[]{:S(2)}) copy-start(bf16[128,96]{0,1:T(8,128)(2,1)} %param.18) | copy-start | bytes 73732
  9.9 22.0 %copy-start.10 = (bf16[128,32]{0,1:T(8,128)(2,1)S(1)}, bf16[128,32]{0,1:T(8,128)(2,1)}, u32[]{:S(2)}) copy-start(bf16[128,32]{0,1:T(8,128)(2,1)} %param.21) | copy-start | bytes 24580
  9.9 304.1 %copy-start.3 = (bf16[256,128]{1,0:T(8,128)(2,1)S(1)}, bf16[256,128]{1,0:T(8,128)(2,1)}, u32[]{:S(2)}) copy-start(bf16[256,128]{1,0:T(8,128)(2,1)} %param.24) | copy-start | bytes 196612
  9.9 304.1 %copy-start.8 = (bf16[256,64]{0,1:T(8,128)(2,1)S(1)}, bf16[256,64]{0,1:T(8,128)(2,1)}, u32[]{:S(2)}) copy-start(bf16[256,64]{0,1:T(8,128)(2,1)} %param.22) | copy-start | bytes 98308
  9.9 304.1 %copy-start.12 = (bf16[256,128]{1,0:T(8,128)(2,1)S(1)}, bf16[256,128]{1,0:T(8,128)(2,1)}, u32[]{:S(2)}) copy-start(bf16[256,128]{1,0:T(8,128)(2,1)} %param.25) | copy-start | bytes 196612
  9.9 304.1 %copy-start.13 = (bf16[256,64]{0,1:T(8,128)(2,1)S(1)}, bf16[256,64]{0,1:T(8,128)(2,1)}, u32[]{:S(2)}) copy-start(bf16[256,64]{0,1:T(8,128)(2,1)} %param.23) | copy-start | bytes 98308
  9.9 304.0 %all-to-all-start = ((bf16[64,128,256]{2,1,0:T(8,128)(2,1)}), bf16[64,128,256]{2,1,0:T(8,128)(2,1)}, u32[]{:S(2)}, u32[]{:S(2)}) async-start(bf16[64,128,256]{2,1,0:T(8,128)(2,1)} %stack.2), calls=%async_computation | async-start | bytes 8388608 | tf_op jit(solution)/shard_map/all_to_all | solution.py:17
  29.6 377.2 %all-gather.2.cloned.1.call-start = ((), (), s32[]{:S(2)}) async-start(), calls=%async_computation.4 | async-start | bytes 9052160 | tf_op jit(solution)/shard_map/all_gather | solution.py:35
  314.0 49.8 %copy-start.2 = (bf16[64,2048]{1,0:T(8,128)(2,1)S(1)}, bf16[64,2048]{1,0:T(8,128)(2,1)}, u32[]{:S(2)}) copy-start(bf16[64,2048]{1,0:T(8,128)(2,1)} %param.26) | copy-start | bytes 786436
  363.8 28.1 %copy-start.11 = (bf16[2048]{0:T(1024)(128)(2,1)S(1)}, bf16[2048]{0:T(1024)(128)(2,1)}, u32[]{:S(2)}) copy-start(bf16[2048]{0:T(1024)(128)(2,1)} %param.28) | copy-start | bytes 12292
  363.8 37.5 %copy-start.1 = (bf16[16,2048]{1,0:T(8,128)(2,1)S(1)}, bf16[16,2048]{1,0:T(8,128)(2,1)}, u32[]{:S(2)}) copy-start(bf16[16,2048]{1,0:T(8,128)(2,1)} %param.17) | copy-start | bytes 196612
  365.4 35.9 %all-to-all-start.1 = ((bf16[8,16,2048]{2,1,0:T(8,128)(2,1)}), bf16[8,16,2048]{2,1,0:T(8,128)(2,1)S(1)}, u32[]{:S(2)}, u32[]{:S(2)}) async-start(bf16[8,16,2048]{2,1,0:T(8,128)(2,1)} %bitcast.22), calls=%async_computation.1 | async-start | bytes 1048576 | tf_op jit(solution)/shard_map/all_to_all | solution.py:28
  402.5 13.7 %all-to-all-start.2 = ((bf16[8,16,2048]{2,1,0:T(8,128)(2,1)}), bf16[8,16,2048]{2,1,0:T(8,128)(2,1)S(1)}, u32[]{:S(2)}, u32[]{:S(2)}) async-start(bf16[8,16,2048]{2,1,0:T(8,128)(2,1)} %broadcast_in_dim.17), calls=%async_computation.2 | async-start | bytes 1048576 | tf_op jit(solution)/shard_map/all_to_all | solution.py:47
Sparse Core Ops, SparseCore 0:
  33.4 240.0 all-gather.1
